TPU v7x, 32 devices: a whole 2x2x4 slice. The times are simulated.
32 devices in a mesh: ep: 8 (over z, core), tp: 4 (over y, x).
Axes of the slice: x: 2, y: 2, z: 4, core: 2. Of those that a mesh axis runs over, the one named last changes fastest.
Arguments:
- query_rows: bfloat16 [4096, 2048], P('ep', 'tp'), may hold values from -6 to 6
- key_rows: bfloat16 [4096, 2048], P('ep', 'tp'), may hold values from -6 to 6
- value_rows: bfloat16 [4096, 4096], P('ep', 'tp'), may hold values from -6 to 6
- in_gate: float32 [16, 4096], P('tp', 'ep'), may hold values from -120 to 120
- forget_gate: float32 [16, 4096], P('tp', 'ep'), may hold values from -2 to 20
- out_gate: bfloat16 [4096, 4096], P('ep', 'tp'), may hold values from -6 to 6
- head_gain: float32 [4096], P('tp'), may hold values from 0.1 to 1.9
- mix_weight: bfloat16 [4096, 4096], P(None, 'tp'), may hold values from -0.09375 to 0.09375
- expert_input: bfloat16 [2048, 4096], P('ep', 'tp'), may hold values from -30 to 30
- routes: int32 [2048, 2], P('ep'), may hold values from 0 to 7, all different within a row; in each aligned block of 256 rows (0 to 255, 256 to 511, ...) at most 128 rows name the same one
- route_weight: float32 [2048, 2], P('ep'), may hold values from 0.25 to 1.25
- gate_weight: bfloat16 [8, 1024, 4096], P('ep', 'tp'), may hold values from -0.09375 to 0.09375
- up_weight: bfloat16 [8, 1024, 4096], P('ep', 'tp'), may hold values from -0.09375 to 0.09375
- down_weight: bfloat16 [8, 1024, 4096], P('ep', None, 'tp'), may hold values from -0.1875 to 0.1875
Outputs:
- mixer_out: bfloat16 [4096, 4096], P('ep', 'tp')
- expert_out: bfloat16 [2048, 4096], P('ep', 'tp')
Inputs may be any that keep to these rules, and one draw needn't show every extreme that they name: `routes`: each row names 2 different experts. In the rows of one device no expert is named by more than 128 rows, and in the rows of some device an expert is named by exactly 128 rows.
All inputs are finite; a program needn't handle non-finite values.
Results may differ from a plain program's by a relative error of at most 0.0057.
Values may be sent and summed in bfloat16 or wider, within the bound.
No kernel may reach another device: no remote copies, remote signals or barrier semaphores. Data moves between devices by JAX's collectives and lax.ppermute only.
A program may use at most 128 MiB of HBM per device.

v0:
```python
import jax
import jax.numpy as jnp
from jax import lax
from jax.sharding import PartitionSpec as P

D = 4096
BLOCK = 64
EPSILON = 1e-06
LOG_FLOOR = -1e30
HIGHEST_PRECISION = lax.Precision.HIGHEST


def carried_in(value, axis, join, neutral):
    count, mine = (lax.axis_size(axis), lax.axis_index(axis))
    pieces = jax.tree.map(lambda part: lax.all_gather(part, axis), value)
    subtotal = jax.tree.map(
        lambda part, zero: jnp.full_like(part, 0) + jnp.asarray(zero, part.dtype), value, neutral
    )

    def turn(position, subtotal):
        longer = join(subtotal, jax.tree.map(lambda part: part[position], pieces))
        return jax.tree.map(lambda new, old: jnp.where(position < mine, new, old), longer, subtotal)

    return lax.fori_loop(0, count - 1, turn, subtotal)


def combine(first_part, second_part):
    decay_first, max_first, memory_first, normal_first = first_part
    decay_second, max_second, memory_second, normal_second = second_part
    running_max = jnp.maximum(decay_second + max_first, max_second)
    keep_first = jnp.exp(decay_second + max_first - running_max)
    keep_second = jnp.exp(max_second - running_max)
    memory = (
        keep_first[..., None, None] * memory_first + keep_second[..., None, None] * memory_second
    )
    normalizer = keep_first[..., None] * normal_first + keep_second[..., None] * normal_second
    return (decay_first + decay_second, running_max, memory, normalizer)


def identity_state(head_count, key_width, value_width):
    return (
        jnp.zeros((head_count,), jnp.float32),
        jnp.full((head_count,), LOG_FLOOR, jnp.float32),
        jnp.zeros((head_count, key_width, value_width), jnp.float32),
        jnp.zeros((head_count, key_width), jnp.float32),
    )


def halfprod(form, left, right):
    return jnp.einsum(form, left, right, preferred_element_type=jnp.float32)


def prepare(query_heads, key_heads, value_heads, in_gate, forget_gate):
    head_count, length, key_width = query_heads.shape
    block_count = length // BLOCK
    query_blocks = query_heads.reshape(head_count, block_count, BLOCK, key_width)
    key_blocks = key_heads.reshape(head_count, block_count, BLOCK, key_width)
    value_blocks = value_heads.reshape(head_count, block_count, BLOCK, value_heads.shape[-1])
    log_input = in_gate.reshape(head_count, block_count, BLOCK)
    cumulative = jnp.cumsum(
        jax.nn.log_sigmoid(forget_gate).reshape(head_count, block_count, BLOCK), axis=-1
    )
    block_decay = cumulative[..., -1]
    weight_log = block_decay[..., None] - cumulative + log_input
    block_max = jnp.max(weight_log, axis=-1)
    weighted = (
        key_blocks.astype(jnp.float32) * jnp.exp(weight_log - block_max[..., None])[..., None]
    )
    normalizer = jnp.sum(weighted, axis=2)
    memory = halfprod("hcsk,hcsv->hckv", weighted.astype(jnp.bfloat16), value_blocks)
    return (
        (query_blocks, key_blocks, value_blocks, log_input, cumulative),
        (block_decay, block_max, memory, normalizer),
    )


def prefix(summary, initial):
    leading = jax.tree.map(lambda tensor: jnp.moveaxis(tensor, 1, 0), summary)

    def advance(running, current):
        return (combine(running, current), running)

    final_state, before = lax.scan(advance, initial, leading)
    return (final_state, jax.tree.map(lambda tensor: jnp.moveaxis(tensor, 0, 1), before))


def block_outputs(blocked, before):
    query_blocks, key_blocks, value_blocks, log_input, cumulative = blocked
    prior_max, prior_memory, prior_normal = (before[1], before[2], before[3])
    block_len = cumulative.shape[-1]
    scale = query_blocks.shape[-1] ** (-0.5)
    causal = jnp.tril(jnp.ones((block_len, block_len), dtype=bool))
    log_decay = jnp.where(
        causal,
        cumulative[..., :, None] - cumulative[..., None, :] + log_input[..., None, :],
        -jnp.inf,
    )
    log_inter = cumulative + prior_max[..., None]
    top_value = jnp.maximum(log_inter, jnp.max(log_decay, axis=-1))
    scores = (
        halfprod("hctk,hcsk->hcts", query_blocks, key_blocks)
        * scale
        * jnp.exp(log_decay - top_value[..., None])
    )
    carried = jnp.exp(log_inter - top_value) * scale
    query_wide = query_blocks.astype(jnp.float32)
    numerator = carried[..., None] * jnp.einsum(
        "hctk,hckv->hctv", query_wide, prior_memory, precision=HIGHEST_PRECISION
    ) + halfprod("hcts,hcsv->hctv", scores.astype(jnp.bfloat16), value_blocks)
    denominator = carried * jnp.einsum(
        "hctk,hck->hct", query_wide, prior_normal, precision=HIGHEST_PRECISION
    ) + jnp.sum(scores, axis=-1)
    return numerator / jnp.maximum(jnp.abs(denominator), jnp.exp(-top_value))[..., None]


def finish(head_values, out_gate, head_gain):
    head_count, block_count, block_len, value_width = head_values.shape
    per_head = jnp.transpose(head_values, (1, 2, 0, 3)).reshape(
        block_count * block_len, head_count, value_width
    )
    per_head = per_head * lax.rsqrt(jnp.mean(per_head * per_head, axis=-1, keepdims=True) + EPSILON)
    per_head = per_head.reshape(block_count * block_len, head_count * value_width) * head_gain
    per_head = per_head * jax.nn.sigmoid(out_gate.astype(jnp.float32))
    return per_head.astype(jnp.bfloat16)


def cell_heads(query_rows, key_rows, value_rows, in_gate, forget_gate, out_gate, head_gain):
    length = query_rows.shape[0]
    head_count = in_gate.shape[0]
    key_width = query_rows.shape[1] // head_count
    value_width = value_rows.shape[1] // head_count
    query_heads = query_rows.reshape(length, head_count, key_width).transpose(1, 0, 2)
    key_heads = key_rows.reshape(length, head_count, key_width).transpose(1, 0, 2)
    value_heads = value_rows.reshape(length, head_count, value_width).transpose(1, 0, 2)
    blocked, summary = prepare(query_heads, key_heads, value_heads, in_gate, forget_gate)
    initial = identity_state(head_count, key_width, value_width)
    final_state, before = prefix(summary, initial)
    incoming = carried_in(final_state, "ep", combine, initial)
    expanded = jax.tree.map(lambda tensor: tensor[:, None], incoming)
    before = combine(expanded, before)
    return finish(block_outputs(blocked, before), out_gate, head_gain)


def body(
    query_rows,
    key_rows,
    value_rows,
    in_gate,
    forget_gate,
    out_gate,
    head_gain,
    mix_weight,
    expert_input,
    routes,
    route_weight,
    gate_weight,
    up_weight,
    down_weight,
):
    mixed_heads = cell_heads(
        query_rows, key_rows, value_rows, in_gate, forget_gate, out_gate, head_gain
    )
    gate_local = gate_weight[0]
    up_local = up_weight[0]
    down_local = down_weight[0]
    group_size = lax.axis_size("ep")
    token_count, fanout = routes.shape
    capacity = 2 * token_count * fanout // group_size
    slot_count = group_size * capacity
    chosen = routes.reshape(-1)
    one_hot = (chosen[:, None] == jnp.arange(group_size, dtype=jnp.int32)[None, :]).astype(
        jnp.int32
    )
    position = jnp.sum((jnp.cumsum(one_hot, axis=0) - one_hot) * one_hot, axis=1)
    target = chosen * capacity + position
    matches = (jnp.arange(slot_count, dtype=jnp.int32)[:, None] == target[None, :]).astype(
        jnp.int32
    )
    occupied = jnp.sum(matches, axis=1) > 0
    source_row = jnp.sum(
        matches * (jnp.arange(token_count * fanout, dtype=jnp.int32) // fanout)[None, :], axis=1
    )
    arrived = lax.all_to_all(
        jnp.where(
            occupied[:, None],
            jnp.take(expert_input, source_row, axis=0),
            jnp.zeros((), expert_input.dtype),
        ),
        "ep",
        split_axis=0,
        concat_axis=0,
        tiled=True,
    )
    head_piece = lax.all_gather(mixed_heads, "tp", axis=1, tiled=True)
    token_piece = lax.all_gather(arrived, "tp", axis=1, tiled=True)
    mix_acc = jnp.dot(head_piece, mix_weight, preferred_element_type=jnp.float32)
    gate_acc = jnp.einsum("sd,fd->sf", token_piece, gate_local, preferred_element_type=jnp.float32)
    up_acc = jnp.einsum("sd,fd->sf", token_piece, up_local, preferred_element_type=jnp.float32)
    squares = jnp.sum(jnp.square(token_piece.astype(jnp.float32)), axis=1)
    mix_acc, gate_acc, up_acc, squares = (mix_acc, gate_acc, up_acc, squares)
    mixer_out = mix_acc.astype(jnp.bfloat16)
    inverse_rms = lax.rsqrt(squares / D + EPSILON)[:, None]
    hidden = (jax.nn.silu(gate_acc * inverse_rms) * (up_acc * inverse_rms)).astype(jnp.bfloat16)
    expert_rows = jnp.dot(
        lax.all_gather(hidden, "tp", axis=1, tiled=True),
        down_local,
        preferred_element_type=jnp.float32,
    )
    returned_rows = lax.all_to_all(
        expert_rows.astype(jnp.bfloat16), "ep", split_axis=0, concat_axis=0, tiled=True
    )
    picked_rows = (
        jnp.take(returned_rows, target, axis=0).reshape(token_count, fanout, -1).astype(jnp.float32)
    )
    expert_out = jnp.sum(picked_rows * route_weight[:, :, None], axis=1).astype(jnp.bfloat16)
    return (mixer_out, expert_out)


def solution(mesh):
    in_specs = (
        P("ep", "tp"),
        P("ep", "tp"),
        P("ep", "tp"),
        P("tp", "ep"),
        P("tp", "ep"),
        P("ep", "tp"),
        P("tp"),
        P(None, "tp"),
        P("ep", "tp"),
        P("ep", None),
        P("ep", None),
        P("ep", "tp", None),
        P("ep", "tp", None),
        P("ep", None, "tp"),
    )
    out_specs = (P("ep", "tp"), P("ep", "tp"))
    return jax.shard_map(body, mesh=mesh, in_specs=in_specs, out_specs=out_specs, check_vma=False)
```

profile of v0, /device:TPU:0, one launch (start us, length us, event | category | flops | bytes accessed | tf_op | source)
XLA Modules:
  0.0 351.7 jit_solution(7868608144681176539)
XLA Ops:
  10.5 2.6 reshape.229
  13.1 2.3 copy.78
  15.4 1.2 reshape.227
  17.1 1.0 copy-done.5
  18.0 3.1 convolution_bitcast_fusion
  21.1 18.0 %while.43 = (s32[]{:T(128)}, f32[4]{0:T(128)S(1)}, f32[4]{0:T(128)S(1)}, f32[4,128,256]{2,1,0:T(8,128)S(1)}, f32[4,128]{1,0:T(4,128)S(1)}, /*index=5*/f32[8,4]{1...) while((s32[]{:T(128)}, f32[4]{0:T(128)S(1)}, ...), condition=%wide.region_4.5_spmd.clone, body=%wide.region_3.4_spmd.clone.sunk | while | flops 657951 | bytes 2636291 | solution.py:83
  22.0 1.2 fusion.83
  24.3 1.2 fusion.83
  26.5 1.2 fusion.83
  28.8 1.2 fusion.83
  31.1 1.2 fusion.83
  33.3 1.2 fusion.83
  35.5 1.2 fusion.83
  37.8 1.2 fusion.83
  40.5 1.1 reduce-window.6
  42.6 5.4 %gather_fusion = bf16[1024,1024]{1,0:T(8,128)(2,1)} fusion(bf16[256,1024]{1,0:T(8,128)(2,1)S(1)} %copy-done.1, s32[1024]{0:T(1024)S(1)} %broadcast_clamp_fusion), kind=kCustom, calls=%fused_computation | custom fusion | bytes 4198400 | tf_op jit(solution)/shard_map/jit(_take)/gather | solution.py:186
  48.0 1.9 select_select_fusion
  49.9 83.4 %all_to_all.21 = bf16[8,128,1024]{2,1,0:T(8,128)(2,1)} all-to-all(bf16[8,128,1024]{2,1,0:T(8,128)(2,1)S(1)} %select_select_fusion), channel_id=1, replica_groups=mesh['ep'=8,'tp'=4] {'ep'}, dimensions={0} | all-to-all | bytes 4194304 | tf_op jit(solution)/shard_map/all_to_all | solution.py:183
  135.6 14.3 %all-reduce.2 = (f32[32]{0:T(128)S(1)}, f32[32]{0:T(128)S(1)}) all-reduce(f32[32]{0:T(128)S(1)} %dynamic-update-slice, f32[32]{0:T(128)S(1)} %dynamic-update-slice.1), channel_id=2, replica_groups=mesh['ep'=8,'tp'=4] {'ep'}, use_global_device_ids=true, to_apply=%add | all-reduce | flops 64 | bytes 512
  151.0 1.1 copy.84
  152.1 13.0 %all-gather.4 = f32[8,4,128]{2,1,0:T(4,128)S(1)} all-gather(f32[1,4,128]{2,1,0:T(4,128)S(1)} %bitcast.238), channel_id=5, replica_groups=mesh['ep'=8,'tp'=4] {'ep'}, dimensions={0}, use_global_device_ids=true | all-gather | bytes 18432 | tf_op jit(solution)/shard_map/all_gather | solution.py:15
  165.7 9.6 %while.44 = (s32[]{:T(128)}, f32[4]{0:T(128)S(1)}, f32[4,128,256]{2,1,0:T(8,128)S(1)}, f32[4,128]{1,0:T(4,128)S(1)}, s32[]{:T(128)}, /*index=5*/f32[8,4]{1,0:T(8...) while((s32[]{:T(128)}, f32[4]{0:T(128)S(1)}, ...), condition=%wide.region_6.7_spmd.clone, body=%wide.region_5.6_spmd.clone.sunk | while | flops 657956 | bytes 1579390 | solution.py:24
  165.8 1.2 fusion.84
  167.1 1.2 fusion.84
  168.4 1.2 fusion.84
  169.8 1.2 fusion.84
  171.1 1.2 fusion.84
  172.4 1.3 fusion.84
  173.9 1.3 fusion.84
  175.4 44.2 %all-gather.12.cloned.1.call-done = bf16[1024,4096]{1,0:T(8,128)(2,1)} async-done(((bf16[1024,1024]{1,0:T(8,128)(2,1)}), bf16[1024,4096]{1,0:T(8,128)(2,1)}) %all-gather.12.cloned.1.call-update) | async-done | bytes 8388624 | tf_op jit(solution)/shard_map/all_gather | solution.py:195
  219.6 5.2 %multiply_reduce_fusion = f32[1024]{0:T(1024)S(1)} fusion(bf16[1024,4096]{1,0:T(8,128)(2,1)} %all-gather.12.cloned.1.call-done), kind=kLoop, calls=%fused_computation.36 | loop fusion | flops 12581888 | bytes 8392704 | tf_op jit(solution)/shard_map/reduce_sum | solution.py:199
  225.4 4.1 %fusion.29 = f32[1024,256]{1,0:T(8,128)S(1)} fusion(bf16[1024,4096]{1,0:T(8,128)(2,1)S(1)} %copy-done.3, bf16[1,256,4096]{2,1,0:T(8,128)(2,1)} %param.29, f32[1024]{0:T(1024)S(1)} %add_rsqrt_fusion.1), kind=kOutput, calls=%fused_computation.63 | convolution fusion | flops 2147745792 | bytes 11538432 | tf_op jit(solution)/shard_map/sd,fd->sf/dot_general | solution.py:197
  229.5 3.3 fusion.38
  234.2 1.7 fusion.65
  236.0 4.4 %fusion.16 = f32[4,8,256,64]{2,3,1,0:T(8,128)S(1)} fusion(bf16[4,8,64,128]{3,2,1,0:T(8,128)(2,1)S(1)} %bitcast.231, f32[8,4,128,256]{3,2,1,0:T(8,128)} %get-tuple-element.240, f32[4,8]{0,1:T(8,128)S(1)} %fusion.58, f32[4,128,256]{2,1,0:T(8,128)S(1)} %get-tuple-element.239, f32[4,8]{0,1:T(8,128)S(1)} %get-tuple-element.432), kind=kOutput, calls=%fused_computation.39 | convolution fusion | flops 808452096 | bytes 7340288 | tf_op jit(solution)/shard_map/hctk,hckv->hctv/dot_general | solution.py:107
  240.4 1.6 multiply_reduce_fusion.2
  242.1 1.4 copy.88
  243.5 1.8 copy.102
  246.6 1.1 copy-done.4
  247.9 1.6 multiply_convert_fusion
  249.6 18.4 %all-gather.14.cloned.1.call-done = bf16[1024,1024]{1,0:T(8,128)(2,1)} async-done(((bf16[1024,256]{1,0:T(8,128)(2,1)}), bf16[1024,1024]{1,0:T(8,128)(2,1)}) %all-gather.14.cloned.1.call-update) | async-done | bytes 2097168 | tf_op jit(solution)/shard_map/all_gather | solution.py:205
  268.0 5.3 %fusion.25 = bf16[1024,1024]{1,0:T(8,128)(2,1)} fusion(bf16[1024,1024]{1,0:T(8,128)(2,1)} %all-gather.14.cloned.1.call-done, bf16[1,1024,1024]{2,1,0:T(8,128)(2,1)S(1)} %copy-done), kind=kOutput, calls=%fused_computation.59 | convolution fusion | flops 2148532224 | bytes 6291456 | tf_op jit(solution)/shard_map/dot_general | solution.py:204
  273.3 4.7 %all-to-all-start.1 = ((bf16[8,128,1024]{2,1,0:T(8,128)(2,1)}), bf16[8,128,1024]{2,1,0:T(8,128)(2,1)}, u32[]{:S(2)}, u32[]{:S(2)}) async-start(bf16[8,128,1024]{2,1,0:T(8,128)(2,1)} %bitcast.232), calls=%async_computation.1 | async-start | bytes 4194304 | tf_op jit(solution)/shard_map/all_to_all | solution.py:209
  278.9 44.0 %all-gather.10.cloned.1.call-done = bf16[512,4096]{1,0:T(8,128)(2,1)} async-done(((bf16[512,1024]{1,0:T(8,128)(2,1)}), bf16[512,4096]{1,0:T(8,128)(2,1)}) %all-gather.10.cloned.1.call-update) | async-done | bytes 4194320 | tf_op jit(solution)/shard_map/all_gather | solution.py:194
  322.9 10.1 %convolution_convert_fusion = bf16[512,1024]{1,0:T(8,128)(2,1)} fusion(bf16[512,4096]{1,0:T(8,128)(2,1)} %all-gather.10.cloned.1.call-done, bf16[4096,1024]{1,0:T(8,128)(2,1)} %param.25), kind=kOutput, calls=%fused_computation.60 | convolution fusion | flops 4295491584 | bytes 13631488 | tf_op jit(solution)/shard_map/dot_general | solution.py:196
  333.0 4.6 %gather_fusion.1 = bf16[512,1024]{1,0:T(8,128)(2,1)S(1)} fusion(bf16[1024,1024]{1,0:T(8,128)(2,1)} %bitcast.39, s32[1024]{0:T(1024)S(1)} %pad_clamp_fusion), kind=kCustom, calls=%fused_computation.1 | custom fusion | bytes 2099200 | tf_op jit(solution)/shard_map/jit(_take)/gather | solution.py:213
  337.6 1.2 gather.15
  338.8 6.3 %multiply_reduce_fusion.1 = bf16[256,1024]{1,0:T(8,128)(2,1)} fusion(bf16[256,2,1024]{2,1,0:T(2,128)(2,1)} %gather.15, pred[256,2]{1,0:T(8,128)(4,1)S(1)} %copy.93, f32[256,2]{1,0:T(8,128)S(1)} %copy.95), kind=kLoop, calls=%fused_computation.51 | loop fusion | flops 1835008 | bytes 1575424 | tf_op jit(solution)/shard_map/reduce_sum | solution.py:215
  (193 shorter events, 23.0 us)
Async XLA Ops:
  7.2 260.8 %copy-start = (bf16[1,1024,1024]{2,1,0:T(8,128)(2,1)S(1)}, bf16[1,1024,1024]{2,1,0:T(8,128)(2,1)}, u32[]{:S(2)}) copy-start(bf16[1,1024,1024]{2,1,0:T(8,128)(2,1)} %param.31) | copy-start | bytes 6291460
  7.2 158.5 %all-gather.16.cloned.1.call-start = ((), (), s32[]{:S(2)}) async-start(), calls=%async_computation.5 | async-start | bytes 4718592 | tf_op jit(solution)/shard_map/all_gather | solution.py:15
  16.6 1.4 copy-start.5
  16.7 4.4 %copy-start.7 = (bf16[4,512,128]{2,1,0:T(8,128)(2,1)}, bf16[4,512,128]{2,1,0:T(8,128)(2,1)S(1)}, u32[]{:S(2)}) copy-start(bf16[4,512,128]{2,1,0:T(8,128)(2,1)S(1)} %copy.77) | copy-start | bytes 1572868
  21.1 18.9 %copy-start.10 = (s32[256,2]{0,1:T(2,128)S(1)}, s32[256,2]{0,1:T(2,128)}, u32[]{:S(2)}) copy-start(s32[256,2]{0,1:T(2,128)} %param.27) | copy-start | bytes 6148
  39.1 0.8 copy-start.2
  39.2 3.5 copy-start.1
  40.0 179.6 %all-gather.12.cloned.1.call-start = ((), (), s32[]{:S(2)}) async-start(), calls=%async_computation.3 | async-start | bytes 10485760 | tf_op jit(solution)/shard_map/all_gather | solution.py:195
  133.2 0.7 copy-start.14
  133.2 16.8 %copy-start.9 = (bf16[512,512]{1,0:T(8,128)(2,1)S(1)}, bf16[512,512]{1,0:T(8,128)(2,1)}, u32[]{:S(2)}) copy-start(bf16[512,512]{1,0:T(8,128)(2,1)} %param.18) | copy-start | bytes 1572868
  133.3 134.7 %all-gather.14.cloned.1.call-start = ((), (), s32[]{:S(2)}) async-start(), calls=%async_computation.4 | async-start | bytes 2621440 | tf_op jit(solution)/shard_map/all_gather | solution.py:205
  219.6 5.8 %copy-start.3 = (bf16[1024,4096]{1,0:T(8,128)(2,1)S(1)}, bf16[1024,4096]{1,0:T(8,128)(2,1)}, u32[]{:S(2)}) copy-start(bf16[1024,4096]{1,0:T(8,128)(2,1)} %all-gather.12.cloned.1.call-done) | copy-start | bytes 25165828
  225.4 4.1 %copy-start.13 = (bf16[1,256,4096]{2,1,0:T(8,128)(2,1)S(1)}, bf16[1,256,4096]{2,1,0:T(8,128)(2,1)}, u32[]{:S(2)}) copy-start(bf16[1,256,4096]{2,1,0:T(8,128)(2,1)} %param.30) | copy-start | bytes 6291460
  232.8 90.1 %all-gather.10.cloned.1.call-start = ((), (), s32[]{:S(2)}) async-start(), calls=%async_computation.2 | async-start | bytes 5242880 | tf_op jit(solution)/shard_map/all_gather | solution.py:194
  236.0 4.4 %copy-start.6 = (bf16[4,512,256]{2,1,0:T(8,128)(2,1)S(1)}, bf16[4,512,256]{2,1,0:T(8,128)(2,1)}, u32[]{:S(2)}) copy-start(bf16[4,512,256]{2,1,0:T(8,128)(2,1)} %copy.78) | copy-start | bytes 3145732
  246.1 1.6 copy-start.4
  246.1 1.8 copy-start.8
  246.1 1.8 copy-start.11
  273.3 5.5 %copy-start.12 = (f32[256,2]{0,1:T(2,128)S(1)}, f32[256,2]{0,1:T(2,128)}, u32[]{:S(2)}) copy-start(f32[256,2]{0,1:T(2,128)} %param.28) | copy-start | bytes 6148
  273.3 59.7 %all-to-all-start.1 = ((bf16[8,128,1024]{2,1,0:T(8,128)(2,1)}), bf16[8,128,1024]{2,1,0:T(8,128)(2,1)}, u32[]{:S(2)}, u32[]{:S(2)}) async-start(bf16[8,128,1024]{2,1,0:T(8,128)(2,1)} %bitcast.232), calls=%async_computation.1 | async-start | bytes 4194304 | tf_op jit(solution)/shard_map/all_to_all | solution.py:209
Sparse Core Ops, SparseCore 0:
  40.1 86.1 all-gather.15
  133.4 86.1 all-gather.11
  232.9 35.0 all-gather.13
  270.3 52.5 all-gather.9
where the time goes:
time: 353 us; the launch traced here: 352 us
  blocking collectives  111 us (31%)
  waiting for transfers between devices  107 us (30%)
  other arithmetic  47 us (13%)
  matrix products  34.5 us (10%)
  local copies, waits for them, and re-layouts  32.5 us (9%)
  between operations  14.9 us (4%)
  starting transfers between devices  5.12 us (1%)
    all_to_all x1, blocking collectives, body(): lax.all_to_all(jnp.where(occupied[:, None], jnp.take(expert_input, source...  83.4 us
    all_gather x1, waiting for transfers between devices, body(): token_piece = lax.all_gather(arrived, 'tp', axis=1, tiled=True)  44.2 us
    all_gather x1, waiting for transfers between devices, body(): head_piece = lax.all_gather(mixed_heads, 'tp', axis=1, tiled=True)  44 us
    all_gather x1, waiting for transfers between devices, body(): lax.all_gather(hidden, 'tp', axis=1, tiled=True)  18.4 us
    unnamed x1, blocking collectives  14.3 us
    all_gather x1, blocking collectives, carried_in(): pieces = jax.tree.map(lambda part: lax.all_gather(part, axis), value)  13 us
    dot_general x1, matrix products, body(): jnp.dot(head_piece, mix_weight, preferred_element_type=jnp.float32)  10.1 us
    add x8, other arithmetic, combine(): keep_first[..., None, None] * memory_first  9.38 us
  transfers between devices with their start and end apart: 5, of which 3 were waited for; matrix products, arithmetic and copies ran while one was open for 16% of the time, Pallas kernels for 0%

commit v1 on v0

--- a/solution.py
+++ b/solution.py
@@ -191,8 +191,11 @@
         concat_axis=0,
         tiled=True,
     )
-    head_piece = lax.all_gather(mixed_heads, "tp", axis=1, tiled=True)
-    token_piece = lax.all_gather(arrived, "tp", axis=1, tiled=True)
+    head_piece, token_piece = jnp.split(
+        lax.all_gather(jnp.concatenate([mixed_heads, arrived], axis=0), "tp", axis=1, tiled=True),
+        [mixed_heads.shape[0]],
+        axis=0,
+    )
     mix_acc = jnp.dot(head_piece, mix_weight, preferred_element_type=jnp.float32)
     gate_acc = jnp.einsum("sd,fd->sf", token_piece, gate_local, preferred_element_type=jnp.float32)
     up_acc = jnp.einsum("sd,fd->sf", token_piece, up_local, preferred_element_type=jnp.float32)

time: 353 us -> 434 us (1.23)
  waiting for transfers between devices: 107 us -> 194 us
  blocking collectives: 111 us -> 91.9 us
  starting transfers between devices: 5.12 us -> 11.6 us
    all_to_all x1 -> x0, blocking collectives: 83.4 us -> none  [body(): lax.all_to_all(jnp.where(occupied[:, None], jnp.take(expert_input, source...]
    unnamed x1, blocking collectives: 14.3 us -> 71.1 us
    all_to_all x1, waiting for transfers between devices: 0.01 us -> 38.1 us  [body(): lax.all_to_all(expert_rows.astype(jnp.bfloat16), 'ep', split_axis=0, conc...]
    all_gather x2 -> x1, waiting for transfers between devices: 88.1 us -> 121 us  [body(): lax.all_gather(jnp.concatenate([mixed_heads, arrived], axis=0), 'tp', axi...]
    all_gather x1, waiting for transfers between devices: 18.4 us -> 35.2 us  [body(): lax.all_gather(hidden, 'tp', axis=1, tiled=True)]
    all_gather x1, blocking collectives: 13 us -> 20.8 us  [carried_in(): pieces = jax.tree.map(lambda part: lax.all_gather(part, axis), value)]
    all_to_all x0 -> x1, starting transfers between devices: none -> 6.55 us  [body(): lax.all_to_all(jnp.where(occupied[:, None], jnp.take(expert_input, source...]
  transfers between devices with their start and end apart: 5 -> 5, of which waited for: 3 -> 3; matrix products, arithmetic and copies ran while one was open for 16% -> 11% of each run, Pallas kernels for 0% -> 0%
where the time goes in v1:
time: 434 us; the launch traced here: 433 us
  waiting for transfers between devices  194 us (45%)
  blocking collectives  91.9 us (21%)
  other arithmetic  50.2 us (12%)
  matrix products  38.3 us (9%)
  local copies, waits for them, and re-layouts  31 us (7%)
  between operations  14.9 us (3%)
  starting transfers between devices  11.6 us (3%)
    all_gather x1, waiting for transfers between devices, body(): lax.all_gather(jnp.concatenate([mixed_heads, arrived], axis=0), 'tp', axi...  121 us
    unnamed x1, blocking collectives  71.1 us
    all_to_all x1, waiting for transfers between devices, body(): lax.all_to_all(expert_rows.astype(jnp.bfloat16), 'ep', split_axis=0, conc...  38.1 us
    all_gather x1, waiting for transfers between devices, body(): lax.all_gather(hidden, 'tp', axis=1, tiled=True)  35.2 us
    all_gather x1, blocking collectives, carried_in(): pieces = jax.tree.map(lambda part: lax.all_gather(part, axis), value)  20.8 us
    dot_general x1, matrix products, body(): jnp.dot(head_piece, mix_weight, preferred_element_type=jnp.float32)  10.1 us
    add x8, other arithmetic, combine(): keep_first[..., None, None] * memory_first  9.34 us
    select_n x14, other arithmetic, turn(): jnp.where(position < mine, new, old)  8.95 us
  transfers between devices with their start and end apart: 5, of which 3 were waited for; matrix products, arithmetic and copies ran while one was open for 11% of the time, Pallas kernels for 0%

profile of v1, /device:TPU:0, one launch (start us, length us, event | category | flops | bytes accessed | tf_op | source)
XLA Modules:
  0.0 432.6 jit_solution(13197494657384588470)
XLA Ops:
  10.3 1.2 reshape.227
  12.3 2.6 reshape.229
  15.0 2.4 copy.78
  17.9 4.5 %convolution_bitcast_fusion = f32[8,4,128,256]{3,2,0,1:T(8,128)} fusion(bf16[4,8,64,256]{3,2,1,0:T(8,128)(2,1)} %bitcast.225, bf16[4,8,64,128]{3,2,1,0:T(8,128)(2,1)} %bitcast.232, f32[4,8,64]{2,1,0:T(8,128)S(1)} %subtract_exponential_fusion.4), kind=kOutput, calls=%fused_computation.48 | convolution fusion | flops 135004160 | bytes 5775360 | tf_op jit(solution)/shard_map/hcsk,hcsv->hckv/dot_general | solution.py:50
  22.4 18.1 %while.43 = (s32[]{:T(128)}, f32[4]{0:T(128)S(1)}, f32[4]{0:T(128)S(1)}, f32[4,128,256]{2,1,0:T(8,128)S(1)}, f32[4,128]{1,0:T(4,128)S(1)}, /*index=5*/f32[8,4]{1...) while((s32[]{:T(128)}, f32[4]{0:T(128)S(1)}, ...), condition=%wide.region_4.5_spmd.clone, body=%wide.region_3.4_spmd.clone.sunk | while | flops 657951 | bytes 2636791 | solution.py:83
  23.3 1.2 fusion.95
  25.5 1.2 fusion.95
  27.8 1.2 fusion.95
  30.1 1.2 fusion.95
  32.3 1.2 fusion.95
  34.6 1.2 fusion.95
  36.8 1.2 fusion.95
  39.1 1.2 fusion.95
  41.7 1.1 reduce-window.6
  43.9 5.4 %gather_fusion = bf16[1024,1024]{1,0:T(8,128)(2,1)} fusion(bf16[256,1024]{1,0:T(8,128)(2,1)S(1)} %copy-done.1, s32[1024]{0:T(1024)S(1)} %broadcast_clamp_fusion), kind=kCustom, calls=%fused_computation | custom fusion | bytes 4198400 | tf_op jit(solution)/shard_map/jit(_take)/gather | solution.py:186
  49.3 2.8 select_select_fusion
  52.1 6.5 %all-to-all-start = ((bf16[8,128,1024]{2,1,0:T(8,128)(2,1)}), bf16[8,128,1024]{2,1,0:T(8,128)(2,1)}, u32[]{:S(2)}, u32[]{:S(2)}) async-start(bf16[8,128,1024]{2,1,0:T(8,128)(2,1)} %select_select_fusion), calls=%async_computation | async-start | bytes 4194304 | tf_op jit(solution)/shard_map/all_to_all | solution.py:183
  60.4 71.1 %all-reduce.2 = (f32[32]{0:T(128)S(1)}, f32[32]{0:T(128)S(1)}) all-reduce(f32[32]{0:T(128)S(1)} %dynamic-update-slice, f32[32]{0:T(128)S(1)} %dynamic-update-slice.1), channel_id=2, replica_groups=mesh['ep'=8,'tp'=4] {'ep'}, use_global_device_ids=true, to_apply=%add | all-reduce | flops 64 | bytes 512
  131.7 0.9 reshape.231
  132.6 1.1 copy.84
  133.7 20.8 %all-gather.4 = f32[8,4,128]{2,1,0:T(4,128)S(1)} all-gather(f32[1,4,128]{2,1,0:T(4,128)S(1)} %bitcast.236), channel_id=5, replica_groups=mesh['ep'=8,'tp'=4] {'ep'}, dimensions={0}, use_global_device_ids=true | all-gather | bytes 18432 | tf_op jit(solution)/shard_map/all_gather | solution.py:15
  155.2 9.3 %while.44 = (s32[]{:T(128)}, f32[4]{0:T(128)S(1)}, f32[4,128,256]{2,1,0:T(8,128)S(1)}, f32[4,128]{1,0:T(4,128)S(1)}, s32[]{:T(128)}, /*index=5*/f32[8,4]{1,0:T(8...) while((s32[]{:T(128)}, f32[4]{0:T(128)S(1)}, ...), condition=%wide.region_6.7_spmd.clone, body=%wide.region_5.6_spmd.clone.sunk | while | flops 657956 | bytes 1579382 | solution.py:24
  155.3 1.2 fusion.96
  156.6 1.2 fusion.96
  157.9 1.2 fusion.96
  159.2 1.2 fusion.96
  160.6 1.2 fusion.96
  161.9 1.2 fusion.96
  163.2 1.2 fusion.96
  164.8 0.9 fusion.68
  165.8 1.7 fusion.80
  167.6 4.4 %fusion.22 = f32[4,8,256,64]{2,3,1,0:T(8,128)S(1)} fusion(bf16[4,8,64,128]{3,2,1,0:T(8,128)(2,1)S(1)} %bitcast.229, f32[8,4,128,256]{3,2,1,0:T(8,128)} %get-tuple-element.240, f32[4,8]{0,1:T(8,128)S(1)} %fusion.73, f32[4,128,256]{2,1,0:T(8,128)S(1)} %get-tuple-element.239, f32[4,8]{0,1:T(8,128)S(1)} %get-tuple-element.432), kind=kOutput, calls=%fused_computation.45 | convolution fusion | flops 808452096 | bytes 7340288 | tf_op jit(solution)/shard_map/hctk,hckv->hctv/dot_general | solution.py:107
  172.0 2.2 multiply_reduce_fusion.2
  175.4 1.1 copy-done.4
  176.5 1.4 copy.88
  179.8 3.6 pad_maximum_fusion
  183.7 120.8 %all-gather.9.cloned.1.call-done = bf16[1536,4096]{1,0:T(8,128)(2,1)} async-done(((bf16[1536,1024]{1,0:T(8,128)(2,1)}), bf16[1536,4096]{1,0:T(8,128)(2,1)}) %all-gather.9.cloned.1.call-update) | async-done | bytes 12582928 | tf_op jit(solution)/shard_map/all_gather | solution.py:195
  304.5 5.2 %multiply_reduce_fusion = f32[1024]{0:T(1024)S(1)} fusion(bf16[1536,4096]{1,0:T(8,128)(2,1)} %all-gather.9.cloned.1.call-done), kind=kLoop, calls=%fused_computation.36 | loop fusion | flops 12581888 | bytes 8392704 | tf_op jit(solution)/shard_map/reduce_sum | solution.py:202
  309.8 5.9 %fusion.36 = f32[1024,256]{1,0:T(8,128)S(1)} fusion(bf16[1,256,4096]{2,1,0:T(8,128)(2,1)S(1)} %copy-done.10, bf16[1536,4096]{1,0:T(8,128)(2,1)} %all-gather.9.cloned.1.call-done, f32[1024]{0:T(1024)S(1)} %add_rsqrt_fusion.1), kind=kOutput, calls=%fused_computation.68 | convolution fusion | flops 2147745792 | bytes 11538432 | tf_op jit(solution)/shard_map/sd,fd->sf/dot_general | solution.py:200
  316.2 3.3 fusion.51
  319.5 35.2 %all-gather.11.cloned.1.call-done = bf16[1024,1024]{1,0:T(8,128)(2,1)} async-done(((bf16[1024,256]{1,0:T(8,128)(2,1)}), bf16[1024,1024]{1,0:T(8,128)(2,1)}) %all-gather.11.cloned.1.call-update) | async-done | bytes 2097168 | tf_op jit(solution)/shard_map/all_gather | solution.py:208
  354.7 5.3 %fusion.29 = bf16[1024,1024]{1,0:T(8,128)(2,1)} fusion(bf16[1024,1024]{1,0:T(8,128)(2,1)} %all-gather.11.cloned.1.call-done, bf16[1,1024,1024]{2,1,0:T(8,128)(2,1)S(1)} %copy-done), kind=kOutput, calls=%fused_computation.64 | convolution fusion | flops 2148532224 | bytes 6291456 | tf_op jit(solution)/shard_map/dot_general | solution.py:207
  360.0 4.7 %all-to-all-start.1 = ((bf16[8,128,1024]{2,1,0:T(8,128)(2,1)}), bf16[8,128,1024]{2,1,0:T(8,128)(2,1)}, u32[]{:S(2)}, u32[]{:S(2)}) async-start(bf16[8,128,1024]{2,1,0:T(8,128)(2,1)} %bitcast.230), calls=%async_computation.1 | async-start | bytes 4194304 | tf_op jit(solution)/shard_map/all_to_all | solution.py:212
  365.6 10.1 %fusion.32 = bf16[512,1024]{1,0:T(8,128)(2,1)} fusion(bf16[4096,1024]{1,0:T(8,128)(2,1)} %param.25, bf16[1536,4096]{1,0:T(8,128)(2,1)} %all-gather.9.cloned.1.call-done), kind=kOutput, calls=%fused_computation.65 | convolution fusion | flops 4295491584 | bytes 13631488 | tf_op jit(solution)/shard_map/dot_general | solution.py:199
  375.8 38.1 %all-to-all-done.1 = bf16[8,128,1024]{2,1,0:T(8,128)(2,1)} async-done(((bf16[8,128,1024]{2,1,0:T(8,128)(2,1)}), bf16[8,128,1024]{2,1,0:T(8,128)(2,1)}, u32[]{:S(2)}, u32[]{:S(2)}) %all-to-all-start.1) | async-done | bytes 2097184 | tf_op jit(solution)/shard_map/all_to_all | solution.py:212
  413.9 4.6 %gather_fusion.1 = bf16[512,1024]{1,0:T(8,128)(2,1)S(1)} fusion(bf16[1024,1024]{1,0:T(8,128)(2,1)} %bitcast.39, s32[1024]{0:T(1024)S(1)} %pad_clamp_fusion), kind=kCustom, calls=%fused_computation.1 | custom fusion | bytes 2099200 | tf_op jit(solution)/shard_map/jit(_take)/gather | solution.py:216
  418.5 1.2 gather.15
  419.7 6.3 %multiply_reduce_fusion.1 = bf16[256,1024]{1,0:T(8,128)(2,1)} fusion(bf16[256,2,1024]{2,1,0:T(2,128)(2,1)} %gather.15, pred[256,2]{1,0:T(8,128)(4,1)S(1)} %copy.93, f32[256,2]{1,0:T(8,128)S(1)} %copy.95), kind=kLoop, calls=%fused_computation.56 | loop fusion | flops 1835008 | bytes 1575424 | tf_op jit(solution)/shard_map/reduce_sum | solution.py:218
  (195 shorter events, 23.0 us)
Async XLA Ops:
  7.2 347.5 %copy-start = (bf16[1,1024,1024]{2,1,0:T(8,128)(2,1)S(1)}, bf16[1,1024,1024]{2,1,0:T(8,128)(2,1)}, u32[]{:S(2)}) copy-start(bf16[1,1024,1024]{2,1,0:T(8,128)(2,1)} %param.31) | copy-start | bytes 6291460
  7.2 148.0 %all-gather.13.cloned.1.call-start = ((), (), s32[]{:S(2)}) async-start(), calls=%async_computation.4 | async-start | bytes 4718592 | tf_op jit(solution)/shard_map/all_gather | solution.py:15
  22.4 18.9 %copy-start.7 = (s32[256,2]{0,1:T(2,128)S(1)}, s32[256,2]{0,1:T(2,128)}, u32[]{:S(2)}) copy-start(s32[256,2]{0,1:T(2,128)} %param.27) | copy-start | bytes 6148
  40.4 0.8 copy-start.2
  40.5 3.4 copy-start.1
  52.1 6.6 %copy-start.12 = (u32[32]{0:T(128)S(1)}, u32[32]{0:T(128)}, u32[]{:S(2)}) copy-start(u32[32]{0:T(128)} %constant.145) | copy-start | bytes 388
  52.1 79.5 %copy-start.6 = (bf16[512,512]{1,0:T(8,128)(2,1)S(1)}, bf16[512,512]{1,0:T(8,128)(2,1)}, u32[]{:S(2)}) copy-start(bf16[512,512]{1,0:T(8,128)(2,1)} %param.18) | copy-start | bytes 1572868
  52.1 127.7 %all-to-all-start = ((bf16[8,128,1024]{2,1,0:T(8,128)(2,1)}), bf16[8,128,1024]{2,1,0:T(8,128)(2,1)}, u32[]{:S(2)}, u32[]{:S(2)}) async-start(bf16[8,128,1024]{2,1,0:T(8,128)(2,1)} %select_select_fusion), calls=%async_computation | async-start | bytes 4194304 | tf_op jit(solution)/shard_map/all_to_all | solution.py:183
  58.7 245.8 %all-gather.9.cloned.1.call-start = ((), (), s32[]{:S(2)}) async-start(), calls=%async_computation.2 | async-start | bytes 15728640 | tf_op jit(solution)/shard_map/all_gather | solution.py:195
  167.5 4.4 %copy-start.3 = (bf16[4,512,256]{2,1,0:T(8,128)(2,1)S(1)}, bf16[4,512,256]{2,1,0:T(8,128)(2,1)}, u32[]{:S(2)}) copy-start(bf16[4,512,256]{2,1,0:T(8,128)(2,1)} %copy.78) | copy-start | bytes 3145732
  174.9 1.6 copy-start.4
  177.9 1.2 copy-start.5
  177.9 1.2 copy-start.8
  183.4 171.3 %all-gather.11.cloned.1.call-start = ((), (), s32[]{:S(2)}) async-start(), calls=%async_computation.3 | async-start | bytes 2621440 | tf_op jit(solution)/shard_map/all_gather | solution.py:208
  304.5 5.2 %copy-start.10 = (bf16[1,256,4096]{2,1,0:T(8,128)(2,1)S(1)}, bf16[1,256,4096]{2,1,0:T(8,128)(2,1)}, u32[]{:S(2)}) copy-start(bf16[1,256,4096]{2,1,0:T(8,128)(2,1)} %param.29) | copy-start | bytes 6291460
  304.5 11.2 %slice-start = ((s8[12582912]{0:T(1024)(128)(4,1)}), s8[4194304]{0:T(1024)(128)(4,1)S(1)}, s32[]{:S(2)}) async-start(s8[12582912]{0:T(1024)(128)(4,1)} %bitcast.220), calls=%async_computation.5 | async-start | bytes 8388608
  309.7 6.0 %slice-start.1 = ((s8[12582912]{0:T(1024)(128)(4,1)}), s8[4194304]{0:T(1024)(128)(4,1)S(1)}, s32[]{:S(2)}) async-start(s8[12582912]{0:T(1024)(128)(4,1)} %bitcast.220), calls=%async_computation.6 | async-start | bytes 8388608
  309.7 6.5 %slice-start.2 = ((s8[12582912]{0:T(1024)(128)(4,1)}), s8[4194304]{0:T(1024)(128)(4,1)S(1)}, s32[]{:S(2)}) async-start(s8[12582912]{0:T(1024)(128)(4,1)} %bitcast.220), calls=%async_computation.7 | async-start | bytes 8388608
  309.7 6.5 %copy-start.11 = (bf16[1,256,4096]{2,1,0:T(8,128)(2,1)S(1)}, bf16[1,256,4096]{2,1,0:T(8,128)(2,1)}, u32[]{:S(2)}) copy-start(bf16[1,256,4096]{2,1,0:T(8,128)(2,1)} %param.30) | copy-start | bytes 6291460
  360.0 5.5 %copy-start.9 = (f32[256,2]{0,1:T(2,128)S(1)}, f32[256,2]{0,1:T(2,128)}, u32[]{:S(2)}) copy-start(f32[256,2]{0,1:T(2,128)} %param.28) | copy-start | bytes 6148
  360.0 53.9 %all-to-all-start.1 = ((bf16[8,128,1024]{2,1,0:T(8,128)(2,1)}), bf16[8,128,1024]{2,1,0:T(8,128)(2,1)}, u32[]{:S(2)}, u32[]{:S(2)}) async-start(bf16[8,128,1024]{2,1,0:T(8,128)(2,1)} %bitcast.230), calls=%async_computation.1 | async-start | bytes 4194304 | tf_op jit(solution)/shard_map/all_to_all | solution.py:212
Sparse Core Ops, SparseCore 0:
  41.4 85.6 all-gather.12
  183.5 120.9 all-gather.8
  319.6 35.0 all-gather.10
